TPU v7x, 32 devices: a whole 2x2x4 slice. The times are simulated.
32 devices in a mesh: fs: 16 (over z, y, core), tp: 2 (over x).
Axes of the slice: x: 2, y: 2, z: 4, core: 2. Of those that a mesh axis runs over, the one named last changes fastest.
Arguments:
- tokens: bfloat16 [6144, 2048], P('fs', 'tp'), may hold values from -60 to 60
- gain_mixer: float32 [2048], P('tp'), may hold values from 0.1 to 1.9
- w_in: bfloat16 [2048, 1024], P('fs', 'tp'), may hold values from -0.125 to 0.125
- pool_scale: float32 [1024], P('tp'), may hold values from 0.1 to 1.9
- w_pool_out: bfloat16 [2048, 1024], P('fs', 'tp'), may hold values from -0.25 to 0.25
- gain_mid: float32 [2048], P('tp'), may hold values from 0.1 to 1.9
- w_ff1: bfloat16 [2048, 8192], P('fs', 'tp'), may hold values from -0.125 to 0.125
- w_ff2: bfloat16 [2048, 8192], P('fs', 'tp'), may hold values from -0.09375 to 0.09375
- gain_out: float32 [2048], P('tp'), may hold values from 0.1 to 1.9
Outputs:
- layer_out: bfloat16 [6144, 2048], P('fs', 'tp')
All inputs are finite; a program needn't handle non-finite values.
Results may differ from a plain program's by a relative error of at most 0.017.
Values may be sent and summed in bfloat16 or wider, within the bound.
A program may use at most 128 MiB of HBM per device.

v0:
```python
import jax
import jax.numpy as jnp
from jax import lax
from jax.sharding import PartitionSpec as P

norm_eps = 1e-05
residual_alpha = 2.0**0.25


def row_norm(value, gain):
    width = value.shape[1] * lax.axis_size("tp")
    total, squares = lax.psum((jnp.sum(value, axis=1), jnp.sum(value * value, axis=1)), "tp")
    mean = (total / width)[:, None]
    spread = (squares / width)[:, None] - mean * mean
    return (value - mean) * lax.rsqrt(spread + norm_eps) * gain


def shifted(value, steps):
    return jnp.pad(value, ((steps, 0), (0, 0)))[: value.shape[0]]


def project_rows(weight, left):
    return lax.dot_general(
        weight, left, (((1,), (1,)), ((), ())), preferred_element_type=jnp.float32
    )


def fold_features(weight, piece):
    return jnp.dot(piece, weight, preferred_element_type=jnp.float32)


def local(tokens, gain_mixer, w_in, pool_scale, w_pool_out, gain_mid, w_ff1, w_ff2, gain_out):
    xf = tokens.astype(jnp.float32)
    length = tokens.shape[0]
    mixed_in = row_norm(xf, gain_mixer).astype(jnp.bfloat16)
    in_full = lax.all_gather(w_in, "fs", axis=0, tiled=True)
    channels = w_in.shape[1]
    pool_in = fold_features(in_full, lax.all_gather(mixed_in, "tp", axis=1, tiled=True))
    uf = pool_in.astype(jnp.bfloat16).astype(jnp.float32)
    group_width = channels * lax.axis_size("tp") // 4
    channel = lax.axis_index("tp") * channels + jnp.arange(channels, dtype=jnp.int32)
    group = channel // group_width
    sum_two = uf + shifted(uf, 1)
    sum_four = sum_two + shifted(sum_two, 2)
    sum_eight = sum_four + shifted(sum_four, 4)
    sum_sixteen = sum_eight + shifted(sum_eight, 8)
    window_sum = jnp.where(
        group == 0,
        sum_two,
        jnp.where(group == 1, sum_four, jnp.where(group == 2, sum_eight, sum_sixteen)),
    )
    window = jnp.where(
        group == 0, 2.0, jnp.where(group == 1, 4.0, jnp.where(group == 2, 8.0, 16.0))
    ).astype(jnp.float32)
    position = jnp.arange(length, dtype=jnp.float32)[:, None]
    count = jnp.minimum(position + 1.0, window[None, :])
    pooled = ((window_sum / count - uf) * pool_scale).astype(jnp.bfloat16)
    out_full = lax.all_gather(w_pool_out, "fs", axis=0, tiled=True)
    mixer_out = lax.psum_scatter(
        project_rows(out_full, pooled).astype(jnp.bfloat16), "tp", scatter_dimension=0, tiled=True
    ).astype(jnp.float32)
    mixer_out = mixer_out.astype(jnp.bfloat16).T
    middle = row_norm(residual_alpha * xf + mixer_out.astype(jnp.float32), gain_mid).astype(
        jnp.bfloat16
    )
    up_full = lax.all_gather(w_ff1, "fs", axis=0, tiled=True)
    upward = fold_features(up_full, lax.all_gather(middle, "tp", axis=1, tiled=True))
    hidden = jnp.square(jax.nn.relu(upward)).astype(jnp.bfloat16)
    down_full = lax.all_gather(w_ff2, "fs", axis=0, tiled=True)
    ff_out = lax.psum_scatter(
        project_rows(down_full, hidden).astype(jnp.bfloat16), "tp", scatter_dimension=0, tiled=True
    ).astype(jnp.float32)
    ff_out = ff_out.astype(jnp.bfloat16).T
    result = row_norm(
        residual_alpha * middle.astype(jnp.float32) + ff_out.astype(jnp.float32), gain_out
    )
    return result.astype(jnp.bfloat16)


def solution(mesh):
    return jax.shard_map(
        local,
        mesh=mesh,
        in_specs=(
            P("fs", "tp"),
            P("tp"),
            P("fs", "tp"),
            P("tp"),
            P("fs", "tp"),
            P("tp"),
            P("fs", "tp"),
            P("fs", "tp"),
            P("tp"),
        ),
        out_specs=P("fs", "tp"),
        check_vma=False,
    )
```

profile of v0, /device:TPU:0, one launch (start us, length us, event | category | flops | bytes accessed | tf_op | source)
XLA Modules:
  0.0 509.2 jit_solution(2410414311106388984)
XLA Ops:
  6.5 1.4 convert_reduce_fusion
  8.0 5.9 %all-reduce.6 = (f32[384]{0:T(512)S(1)}, f32[384]{0:T(512)S(1)}) all-reduce(f32[384]{0:T(512)S(1)} %get-tuple-element.10, f32[384]{0:T(512)S(1)} %get-tuple-element.9), channel_id=1, replica_groups=mesh['fs'=16,'tp'=2] {'tp'}, use_global_device_ids=true, to_apply=%region_3.0 | all-reduce | flops 768 | bytes 6144 | tf_op jit(solution)/shard_map/psum | solution.py:12
  13.9 2.3 fusion.7
  16.2 0.0 all-gather.9.cloned.1.call-start
  16.3 0.7 all-gather.9.cloned.1.call-update
  17.0 0.7 all-gather.11.cloned.1.call-update
  17.7 0.0 reduce-scatter.3.cloned.1.call-start
  17.8 27.5 %all-gather.7.cloned.1.call-done = bf16[384,2048]{1,0:T(8,128)(2,1)} async-done(((bf16[384,1024]{1,0:T(8,128)(2,1)}), bf16[384,2048]{1,0:T(8,128)(2,1)}) %all-gather.7.cloned.1.call-update) | async-done | bytes 1572880 | tf_op jit(solution)/shard_map/all_gather | solution.py:38
  45.3 43.7 %all-gather.9.cloned.1.call-done = bf16[2048,512]{1,0:T(8,128)(2,1)} async-done(((bf16[128,512]{1,0:T(8,128)(2,1)}), bf16[2048,512]{1,0:T(8,128)(2,1)}) %all-gather.9.cloned.1.call-update) | async-done | bytes 2097168 | tf_op jit(solution)/shard_map/all_gather | solution.py:36
  89.0 3.0 fusion.9
  92.0 0.1 fusion.12
  92.2 0.1 fusion.13
  92.3 0.1 fusion.14
  92.4 39.0 %all-gather.11.cloned.1.call-done = bf16[2048,512]{1,0:T(8,128)(2,1)} async-done(((bf16[128,512]{1,0:T(8,128)(2,1)}), bf16[2048,512]{1,0:T(8,128)(2,1)}) %all-gather.11.cloned.1.call-update) | async-done | bytes 2097168 | tf_op jit(solution)/shard_map/all_gather | solution.py:58
  131.4 3.9 fusion.2
  135.3 0.0 all-gather.13.cloned.1.call-start
  135.4 25.0 %reduce-scatter.3.cloned.1.call-done = bf16[1024,384]{0,1:T(8,128)(2,1)} async-done(((bf16[2048,384]{0,1:T(8,128)(2,1)}), bf16[1024,384]{0,1:T(8,128)(2,1)}) %reduce-scatter.3.cloned.1.call-update) | async-done | bytes 786448 | tf_op jit(solution)/shard_map/reduce_scatter | solution.py:59
  160.4 1.7 fusion.11
  162.0 4.9 all-reduce.5
  167.0 1.3 multiply_convert_fusion.2
  168.3 0.0 all-gather.15.cloned.1.call-start
  168.3 0.5 all-gather.15.cloned.1.call-update
  168.9 0.7 all-gather.17.cloned.1.call-update
  169.6 0.0 reduce-scatter.5.cloned.1.call-start
  169.7 26.0 %all-gather.13.cloned.1.call-done = bf16[384,2048]{1,0:T(8,128)(2,1)} async-done(((bf16[384,1024]{1,0:T(8,128)(2,1)}), bf16[384,2048]{1,0:T(8,128)(2,1)}) %all-gather.13.cloned.1.call-update) | async-done | bytes 1572880 | tf_op jit(solution)/shard_map/all_gather | solution.py:67
  195.6 128.5 %all-gather.15.cloned.1.call-done = bf16[2048,4096]{1,0:T(8,128)(2,1)} async-done(((bf16[128,4096]{1,0:T(8,128)(2,1)}), bf16[2048,4096]{1,0:T(8,128)(2,1)}) %all-gather.15.cloned.1.call-update) | async-done | bytes 16777232 | tf_op jit(solution)/shard_map/all_gather | solution.py:66
  324.1 126.8 %all-gather.17.cloned.1.call-done = bf16[2048,4096]{1,0:T(8,128)(2,1)} async-done(((bf16[128,4096]{1,0:T(8,128)(2,1)}), bf16[2048,4096]{1,0:T(8,128)(2,1)}) %all-gather.17.cloned.1.call-update) | async-done | bytes 16777232 | tf_op jit(solution)/shard_map/all_gather | solution.py:69
  450.9 19.0 %fusion.3 = bf16[2048,384]{0,1:T(8,128)(2,1)} fusion(bf16[2048,4096]{1,0:T(8,128)(2,1)} %all-gather.17.cloned.1.call-done, bf16[384,2048]{1,0:T(8,128)(2,1)} %all-gather.13.cloned.1.call-done, bf16[2048,4096]{1,0:T(8,128)(2,1)} %all-gather.15.cloned.1.call-done), kind=kOutput, calls=%fused_computation.9 | convolution fusion | flops 12890406912 | bytes 36700160 | tf_op jit(solution)/shard_map/dot_general | solution.py:23
  470.0 24.5 %reduce-scatter.5.cloned.1.call-done = bf16[1024,384]{0,1:T(8,128)(2,1)} async-done(((bf16[2048,384]{0,1:T(8,128)(2,1)}), bf16[1024,384]{0,1:T(8,128)(2,1)}) %reduce-scatter.5.cloned.1.call-update) | async-done | bytes 786448 | tf_op jit(solution)/shard_map/reduce_scatter | solution.py:70
  494.4 1.7 fusion.10
  496.1 4.9 all-reduce.4
  501.1 1.3 multiply_convert_fusion.1
  (28 shorter events, 0.3 us)
Async XLA Ops:
  6.5 38.8 %all-gather.7.cloned.1.call-start = ((), (), s32[]{:S(2)}) async-start(), calls=%async_computation.2 | async-start | bytes 2359296 | tf_op jit(solution)/shard_map/all_gather | solution.py:38
  16.2 72.8 %all-gather.9.cloned.1.call-start = ((), (), s32[]{:S(2)}) async-start(), calls=%async_computation.3 | async-start | bytes 2228224 | tf_op jit(solution)/shard_map/all_gather | solution.py:36
  17.0 114.4 %all-gather.11.cloned.1.call-start = ((), (), s32[]{:S(2)}) async-start(), calls=%async_computation.4 | async-start | bytes 2228224 | tf_op jit(solution)/shard_map/all_gather | solution.py:58
  17.7 142.7 %reduce-scatter.3.cloned.1.call-start = ((), (), s32[]{:S(2)}) async-start(), calls=%async_computation.5 | async-start | bytes 2359296 | tf_op jit(solution)/shard_map/reduce_scatter | solution.py:59
  92.2 39.2 %copy-start.6 = (f32[512]{0:T(512)S(1)}, f32[512]{0:T(512)}, u32[]{:S(2)}) copy-start(f32[512]{0:T(512)} %param.12) | copy-start | bytes 6148
  135.3 25.0 %copy-start = (bf16[384,1024]{1,0:T(8,128)(2,1)S(1)}, bf16[384,1024]{1,0:T(8,128)(2,1)}, u32[]{:S(2)}) copy-start(bf16[384,1024]{1,0:T(8,128)(2,1)} %param.9) | copy-start | bytes 2359300
  135.3 31.6 %copy-start.4 = (f32[1024]{0:T(1024)S(1)}, f32[1024]{0:T(1024)}, u32[]{:S(2)}) copy-start(f32[1024]{0:T(1024)} %param.14) | copy-start | bytes 12292
  135.3 60.3 %all-gather.13.cloned.1.call-start = ((), (), s32[]{:S(2)}) async-start(), calls=%async_computation.6 | async-start | bytes 2359296 | tf_op jit(solution)/shard_map/all_gather | solution.py:67
  160.3 6.6 %copy-start.2 = (bf16[1024,384]{0,1:T(8,128)(2,1)S(1)}, bf16[1024,384]{0,1:T(8,128)(2,1)}, u32[]{:S(2)}) copy-start(bf16[1024,384]{0,1:T(8,128)(2,1)} %reduce-scatter.3.cloned.1.call-done) | copy-start | bytes 2359300
  168.3 155.8 %all-gather.15.cloned.1.call-start = ((), (), s32[]{:S(2)}) async-start(), calls=%async_computation.7 | async-start | bytes 17825792 | tf_op jit(solution)/shard_map/all_gather | solution.py:66
  168.9 282.1 %all-gather.17.cloned.1.call-start = ((), (), s32[]{:S(2)}) async-start(), calls=%async_computation.8 | async-start | bytes 17825792 | tf_op jit(solution)/shard_map/all_gather | solution.py:69
  169.6 324.8 %reduce-scatter.5.cloned.1.call-start = ((), (), s32[]{:S(2)}) async-start(), calls=%async_computation.9 | async-start | bytes 2359296 | tf_op jit(solution)/shard_map/reduce_scatter | solution.py:70
  469.9 24.5 %copy-start.1 = (bf16[384,1024]{1,0:T(8,128)(2,1)S(1)}, bf16[384,1024]{1,0:T(8,128)(2,1)}, u32[]{:S(2)}) copy-start(bf16[384,1024]{1,0:T(8,128)(2,1)} %multiply_convert_fusion.2) | copy-start | bytes 2359300
  469.9 31.1 %copy-start.5 = (f32[1024]{0:T(1024)S(1)}, f32[1024]{0:T(1024)}, u32[]{:S(2)}) copy-start(f32[1024]{0:T(1024)} %param.17) | copy-start | bytes 12292
  494.4 6.6 %copy-start.3 = (bf16[1024,384]{0,1:T(8,128)(2,1)S(1)}, bf16[1024,384]{0,1:T(8,128)(2,1)}, u32[]{:S(2)}) copy-start(bf16[1024,384]{0,1:T(8,128)(2,1)} %reduce-scatter.5.cloned.1.call-done) | copy-start | bytes 2359300
Sparse Core Ops, SparseCore 0:
  16.3 28.9 all-gather.6
  47.5 41.4 all-gather.8
  91.2 40.1 all-gather.10
  135.5 24.8 reduce-scatter.2
  168.4 27.1 all-gather.12
  197.7 126.4 all-gather.14
  326.3 124.5 all-gather.16
  470.1 24.3 reduce-scatter.4
where the time goes:
time: 510 us; the launch traced here: 509 us
  waiting for transfers between devices  444 us (87%)
  matrix products  26 us (5%)
  blocking collectives  15.7 us (3%)
  between operations  13.6 us (3%)
  other arithmetic  10 us (2%)
    all_gather x1, waiting for transfers between devices, local(): up_full = lax.all_gather(w_ff1, 'fs', axis=0, tiled=True)  128 us
    all_gather x1, waiting for transfers between devices, local(): down_full = lax.all_gather(w_ff2, 'fs', axis=0, tiled=True)  127 us
    all_gather x1, waiting for transfers between devices, local(): in_full = lax.all_gather(w_in, 'fs', axis=0, tiled=True)  43.7 us
    all_gather x1, waiting for transfers between devices, local(): out_full = lax.all_gather(w_pool_out, 'fs', axis=0, tiled=True)  39 us
    all_gather x1, waiting for transfers between devices, local(): lax.all_gather(mixed_in, 'tp', axis=1, tiled=True)  27.5 us
    all_gather x1, waiting for transfers between devices, local(): lax.all_gather(middle, 'tp', axis=1, tiled=True)  26 us
    reduce_scatter x1, waiting for transfers between devices, local(): lax.psum_scatter(project_rows(out_full, pooled).astype(jnp.bfloat16), 'tp...  25 us
    reduce_scatter x1, waiting for transfers between devices, local(): lax.psum_scatter(project_rows(down_full, hidden).astype(jnp.bfloat16), 't...  24.5 us
  transfers between devices with their start and end apart: 8, of which 8 were waited for; matrix products, arithmetic and copies ran while one was open for 1% of the time, Pallas kernels for 0%

commit v1 on v0

--- a/solution.py
+++ b/solution.py
@@ -35,7 +35,7 @@
     mixed_in = row_norm(xf, gain_mixer).astype(jnp.bfloat16)
     in_full = lax.all_gather(w_in, "fs", axis=0, tiled=True)
     channels = w_in.shape[1]
-    pool_in = fold_features(in_full, lax.all_gather(mixed_in, "tp", axis=1, tiled=True))
+    pool_in = fold_features(in_full, jnp.concatenate(lax.all_gather(mixed_in, "tp"), axis=1))
     uf = pool_in.astype(jnp.bfloat16).astype(jnp.float32)
     group_width = channels * lax.axis_size("tp") // 4
     channel = lax.axis_index("tp") * channels + jnp.arange(channels, dtype=jnp.int32)

time: 510 us -> 510 us (level)
  no operation moved by 1% of the time
where the time goes in v1:
time: 510 us; the launch traced here: 509 us
  waiting for transfers between devices  442 us (87%)
  matrix products  25.5 us (5%)
  blocking collectives  15.7 us (3%)
  between operations  13.6 us (3%)
  other arithmetic  10 us (2%)
    all_gather x1, waiting for transfers between devices, local(): up_full = lax.all_gather(w_ff1, 'fs', axis=0, tiled=True)  128 us
    all_gather x1, waiting for transfers between devices, local(): down_full = lax.all_gather(w_ff2, 'fs', axis=0, tiled=True)  127 us
    all_gather x1, waiting for transfers between devices, local(): in_full = lax.all_gather(w_in, 'fs', axis=0, tiled=True)  41.8 us
    all_gather x1, waiting for transfers between devices, local(): out_full = lax.all_gather(w_pool_out, 'fs', axis=0, tiled=True)  39.4 us
    all_gather x1, waiting for transfers between devices, local(): lax.all_gather(mixed_in, 'tp')  27.5 us
    all_gather x1, waiting for transfers between devices, local(): lax.all_gather(middle, 'tp', axis=1, tiled=True)  26 us
    reduce_scatter x1, waiting for transfers between devices, local(): lax.psum_scatter(project_rows(out_full, pooled).astype(jnp.bfloat16), 'tp...  25 us
    reduce_scatter x1, waiting for transfers between devices, local(): lax.psum_scatter(project_rows(down_full, hidden).astype(jnp.bfloat16), 't...  24.5 us
  transfers between devices with their start and end apart: 8, of which 8 were waited for; matrix products, arithmetic and copies ran while one was open for 1% of the time, Pallas kernels for 0%

profile of v1, /device:TPU:0, one launch (start us, length us, event | category | flops | bytes accessed | tf_op | source)
XLA Modules:
  0.0 509.2 jit_solution(2970050344120722175)
XLA Ops:
  6.5 1.4 convert_reduce_fusion
  8.0 5.9 %all-reduce.6 = (f32[384]{0:T(512)S(1)}, f32[384]{0:T(512)S(1)}) all-reduce(f32[384]{0:T(512)S(1)} %get-tuple-element.10, f32[384]{0:T(512)S(1)} %get-tuple-element.9), channel_id=1, replica_groups=mesh['fs'=16,'tp'=2] {'tp'}, use_global_device_ids=true, to_apply=%region_3.0 | all-reduce | flops 768 | bytes 6144 | tf_op jit(solution)/shard_map/psum | solution.py:12
  13.9 2.3 fusion.7
  16.2 0.0 all-gather.8.cloned.1.call-start
  16.3 0.7 all-gather.8.cloned.1.call-update
  17.0 0.7 all-gather.10.cloned.1.call-update
  17.8 27.5 %all-gather.18.cloned.1.call-done = bf16[768,1024]{1,0:T(8,128)(2,1)} async-done(((bf16[384,1024]{1,0:T(8,128)(2,1)}), bf16[768,1024]{1,0:T(8,128)(2,1)}) %all-gather.18.cloned.1.call-update) | async-done | bytes 1572880 | tf_op jit(solution)/shard_map/all_gather | solution.py:38
  45.3 1.9 copy.10
  47.2 41.8 %all-gather.8.cloned.1.call-done = bf16[2048,512]{1,0:T(8,128)(2,1)} async-done(((bf16[128,512]{1,0:T(8,128)(2,1)}), bf16[2048,512]{1,0:T(8,128)(2,1)}) %all-gather.8.cloned.1.call-update) | async-done | bytes 2097168 | tf_op jit(solution)/shard_map/all_gather | solution.py:36
  89.0 2.6 fusion.9
  91.6 0.1 fusion.12
  91.7 0.1 fusion.13
  91.8 0.1 fusion.14
  91.9 39.4 %all-gather.10.cloned.1.call-done = bf16[2048,512]{1,0:T(8,128)(2,1)} async-done(((bf16[128,512]{1,0:T(8,128)(2,1)}), bf16[2048,512]{1,0:T(8,128)(2,1)}) %all-gather.10.cloned.1.call-update) | async-done | bytes 2097168 | tf_op jit(solution)/shard_map/all_gather | solution.py:58
  131.4 3.9 fusion.2
  135.3 0.0 all-gather.12.cloned.1.call-start
  135.4 25.0 %reduce-scatter.3.cloned.1.call-done = bf16[1024,384]{0,1:T(8,128)(2,1)} async-done(((bf16[2048,384]{0,1:T(8,128)(2,1)}), bf16[1024,384]{0,1:T(8,128)(2,1)}) %reduce-scatter.3.cloned.1.call-update) | async-done | bytes 786448 | tf_op jit(solution)/shard_map/reduce_scatter | solution.py:59
  160.4 1.7 fusion.11
  162.0 4.9 all-reduce.5
  167.0 1.3 multiply_convert_fusion.2
  168.3 0.0 all-gather.14.cloned.1.call-start
  168.3 0.5 all-gather.14.cloned.1.call-update
  168.9 0.7 all-gather.16.cloned.1.call-update
  169.6 0.0 reduce-scatter.5.cloned.1.call-start
  169.7 26.0 %all-gather.12.cloned.1.call-done = bf16[384,2048]{1,0:T(8,128)(2,1)} async-done(((bf16[384,1024]{1,0:T(8,128)(2,1)}), bf16[384,2048]{1,0:T(8,128)(2,1)}) %all-gather.12.cloned.1.call-update) | async-done | bytes 1572880 | tf_op jit(solution)/shard_map/all_gather | solution.py:67
  195.7 128.5 %all-gather.14.cloned.1.call-done = bf16[2048,4096]{1,0:T(8,128)(2,1)} async-done(((bf16[128,4096]{1,0:T(8,128)(2,1)}), bf16[2048,4096]{1,0:T(8,128)(2,1)}) %all-gather.14.cloned.1.call-update) | async-done | bytes 16777232 | tf_op jit(solution)/shard_map/all_gather | solution.py:66
  324.1 126.8 %all-gather.16.cloned.1.call-done = bf16[2048,4096]{1,0:T(8,128)(2,1)} async-done(((bf16[128,4096]{1,0:T(8,128)(2,1)}), bf16[2048,4096]{1,0:T(8,128)(2,1)}) %all-gather.16.cloned.1.call-update) | async-done | bytes 16777232 | tf_op jit(solution)/shard_map/all_gather | solution.py:69
  450.9 19.0 %fusion.3 = bf16[2048,384]{0,1:T(8,128)(2,1)} fusion(bf16[2048,4096]{1,0:T(8,128)(2,1)} %all-gather.16.cloned.1.call-done, bf16[384,2048]{1,0:T(8,128)(2,1)} %all-gather.12.cloned.1.call-done, bf16[2048,4096]{1,0:T(8,128)(2,1)} %all-gather.14.cloned.1.call-done), kind=kOutput, calls=%fused_computation.9 | convolution fusion | flops 12890406912 | bytes 36700160 | tf_op jit(solution)/shard_map/dot_general | solution.py:23
  470.0 24.5 %reduce-scatter.5.cloned.1.call-done = bf16[1024,384]{0,1:T(8,128)(2,1)} async-done(((bf16[2048,384]{0,1:T(8,128)(2,1)}), bf16[1024,384]{0,1:T(8,128)(2,1)}) %reduce-scatter.5.cloned.1.call-update) | async-done | bytes 786448 | tf_op jit(solution)/shard_map/reduce_scatter | solution.py:70
  494.5 1.7 fusion.10
  496.1 4.9 all-reduce.4
  501.1 1.3 multiply_convert_fusion.1
  (29 shorter events, 0.3 us)
Async XLA Ops:
  6.5 38.8 %all-gather.18.cloned.1.call-start = ((), (), s32[]{:S(2)}) async-start(), calls=%async_computation.9 | async-start | bytes 2359296 | tf_op jit(solution)/shard_map/all_gather | solution.py:38
  16.2 72.8 %all-gather.8.cloned.1.call-start = ((), (), s32[]{:S(2)}) async-start(), calls=%async_computation.2 | async-start | bytes 2228224 | tf_op jit(solution)/shard_map/all_gather | solution.py:36
  17.0 114.4 %all-gather.10.cloned.1.call-start = ((), (), s32[]{:S(2)}) async-start(), calls=%async_computation.3 | async-start | bytes 2228224 | tf_op jit(solution)/shard_map/all_gather | solution.py:58
  17.7 142.7 %reduce-scatter.3.cloned.1.call-start = ((), (), s32[]{:S(2)}) async-start(), calls=%async_computation.4 | async-start | bytes 2359296 | tf_op jit(solution)/shard_map/reduce_scatter | solution.py:59
  91.7 39.7 %copy-start.6 = (f32[512]{0:T(512)S(1)}, f32[512]{0:T(512)}, u32[]{:S(2)}) copy-start(f32[512]{0:T(512)} %param.12) | copy-start | bytes 6148
  135.3 25.0 %copy-start = (bf16[384,1024]{1,0:T(8,128)(2,1)S(1)}, bf16[384,1024]{1,0:T(8,128)(2,1)}, u32[]{:S(2)}) copy-start(bf16[384,1024]{1,0:T(8,128)(2,1)} %param.9) | copy-start | bytes 2359300
  135.3 31.6 %copy-start.4 = (f32[1024]{0:T(1024)S(1)}, f32[1024]{0:T(1024)}, u32[]{:S(2)}) copy-start(f32[1024]{0:T(1024)} %param.14) | copy-start | bytes 12292
  135.3 60.3 %all-gather.12.cloned.1.call-start = ((), (), s32[]{:S(2)}) async-start(), calls=%async_computation.5 | async-start | bytes 2359296 | tf_op jit(solution)/shard_map/all_gather | solution.py:67
  160.4 6.6 %copy-start.2 = (bf16[1024,384]{0,1:T(8,128)(2,1)S(1)}, bf16[1024,384]{0,1:T(8,128)(2,1)}, u32[]{:S(2)}) copy-start(bf16[1024,384]{0,1:T(8,128)(2,1)} %reduce-scatter.3.cloned.1.call-done) | copy-start | bytes 2359300
  168.3 155.8 %all-gather.14.cloned.1.call-start = ((), (), s32[]{:S(2)}) async-start(), calls=%async_computation.6 | async-start | bytes 17825792 | tf_op jit(solution)/shard_map/all_gather | solution.py:66
  168.9 282.1 %all-gather.16.cloned.1.call-start = ((), (), s32[]{:S(2)}) async-start(), calls=%async_computation.7 | async-start | bytes 17825792 | tf_op jit(solution)/shard_map/all_gather | solution.py:69
  169.6 324.8 %reduce-scatter.5.cloned.1.call-start = ((), (), s32[]{:S(2)}) async-start(), calls=%async_computation.8 | async-start | bytes 2359296 | tf_op jit(solution)/shard_map/reduce_scatter | solution.py:70
  469.9 24.5 %copy-start.1 = (bf16[384,1024]{1,0:T(8,128)(2,1)S(1)}, bf16[384,1024]{1,0:T(8,128)(2,1)}, u32[]{:S(2)}) copy-start(bf16[384,1024]{1,0:T(8,128)(2,1)} %multiply_convert_fusion.2) | copy-start | bytes 2359300
  469.9 31.1 %copy-start.5 = (f32[1024]{0:T(1024)S(1)}, f32[1024]{0:T(1024)}, u32[]{:S(2)}) copy-start(f32[1024]{0:T(1024)} %param.17) | copy-start | bytes 12292
  494.5 6.6 %copy-start.3 = (bf16[1024,384]{0,1:T(8,128)(2,1)S(1)}, bf16[1024,384]{0,1:T(8,128)(2,1)}, u32[]{:S(2)}) copy-start(bf16[1024,384]{0,1:T(8,128)(2,1)} %reduce-scatter.5.cloned.1.call-done) | copy-start | bytes 2359300
Sparse Core Ops, SparseCore 0:
  16.3 28.9 all-gather.17
  47.5 41.4 all-gather.7
  91.2 40.1 all-gather.9
  135.5 24.8 reduce-scatter.2
  168.4 27.1 all-gather.11
  197.7 126.4 all-gather.13
  326.3 124.5 all-gather.15
  470.1 24.3 reduce-scatter.4
